TPU v7x, 32 devices: a whole 2x2x4 slice. The times are simulated.
32 devices in a mesh: fs: 8 (over z, x), tp: 4 (over y, core).
Axes of the slice: x: 2, y: 2, z: 4, core: 2. Of those that a mesh axis runs over, the one named last changes fastest.
Arguments:
- tokens: bfloat16 [16, 384, 2048], P('fs', None, 'tp'), may hold values from -20 to 20
- first_gain: float32 [2048], replicated, may hold values from 0.1 to 1.9
- first_gate: bfloat16 [2048, 5120], P('fs', 'tp'), may hold values from -0.125 to 0.125
- first_up: bfloat16 [2048, 5120], P('fs', 'tp'), may hold values from -0.125 to 0.125
- first_down: bfloat16 [5120, 2048], P('tp', 'fs'), may hold values from -0.078125 to 0.078125
- mixer_gain: float32 [2048], replicated, may hold values from 0.1 to 1.9
- conv_input: bfloat16 [2048, 1024], P('fs', 'tp'), may hold values from -0.125 to 0.125
- outer_gate: bfloat16 [2048, 1024], P('fs', 'tp'), may hold values from -0.125 to 0.125
- inner_gate: bfloat16 [2048, 1024], P('fs', 'tp'), may hold values from -0.125 to 0.125
- conv_taps: float32 [3, 1024], P(None, 'tp'), may hold values from -3.5 to 3.5
- mixer_out: bfloat16 [1024, 2048], P('tp', 'fs'), may hold values from -0.1875 to 0.1875
- second_gain: float32 [2048], replicated, may hold values from 0.1 to 1.9
- second_gate: bfloat16 [2048, 5120], P('fs', 'tp'), may hold values from -0.125 to 0.125
- second_up: bfloat16 [2048, 5120], P('fs', 'tp'), may hold values from -0.125 to 0.125
- second_down: bfloat16 [5120, 2048], P('tp', 'fs'), may hold values from -0.078125 to 0.078125
Outputs:
- layer_out: bfloat16 [16, 384, 2048], P('fs', None, 'tp')
All inputs are finite; a program needn't handle non-finite values.
Results may differ from a plain program's by a relative error of at most 0.015.
Values may be sent and summed in bfloat16 or wider, within the bound.
A program may use at most 64 MiB of HBM per device.

v0:
```python
import jax
import jax.numpy as jnp
from jax import lax
from jax.sharding import PartitionSpec as P

epsilon = 1e-05


def norm_rows(stream, gain):
    whole = lax.all_gather(stream, "tp", axis=1, tiled=True)
    values = whole.astype(jnp.float32)
    scale = lax.rsqrt(jnp.mean(values * values, axis=1, keepdims=True) + epsilon)
    return (values * scale * gain).astype(jnp.bfloat16)


def add_rows(gathered, piece):
    return jnp.dot(gathered, piece, preferred_element_type=jnp.float32)


def ffn_inputs(gathered, gate_weight, up_weight):
    empty = jnp.zeros((gathered.shape[0], gate_weight.shape[1]), jnp.float32)

    def add_single(total, piece, start):
        return add_rows(gathered, piece)

    gate = add_single(empty, lax.all_gather(gate_weight, "fs", axis=0, tiled=True), jnp.int32(0))
    upward = add_single(empty, lax.all_gather(up_weight, "fs", axis=0, tiled=True), jnp.int32(0))
    return (gate, upward)


def mixer_inputs(gathered, conv_input, outer_gate, inner_gate):
    empty = jnp.zeros((gathered.shape[0], conv_input.shape[1]), jnp.float32)

    def add_single(total, piece, start):
        return add_rows(gathered, piece)

    conv_values = add_single(
        empty, lax.all_gather(conv_input, "fs", axis=0, tiled=True), jnp.int32(0)
    )
    outer = add_single(empty, lax.all_gather(outer_gate, "fs", axis=0, tiled=True), jnp.int32(0))
    inner = add_single(empty, lax.all_gather(inner_gate, "fs", axis=0, tiled=True), jnp.int32(0))
    return (conv_values, outer, inner)


def project_down(hidden, weight):
    partial_sum = jnp.dot(
        hidden, lax.all_gather(weight, "fs", axis=1, tiled=True), preferred_element_type=jnp.float32
    )
    result = lax.psum_scatter(
        partial_sum.astype(jnp.bfloat16), "tp", scatter_dimension=1, tiled=True
    ).astype(jnp.float32)
    return result


def half_ffn(stream, gain, gate_weight, up_weight, down_weight):
    gathered = norm_rows(stream, gain)
    gate, upward = ffn_inputs(gathered, gate_weight, up_weight)
    hidden = (jax.nn.silu(gate) * upward).astype(jnp.bfloat16)
    branch = project_down(hidden, down_weight)
    return (stream.astype(jnp.float32) + 0.5 * branch).astype(jnp.bfloat16)


def conv_mixer(stream, seqs, gain, conv_input, outer_gate, inner_gate, conv_taps, mixer_out):
    gathered = norm_rows(stream, gain)
    conv_values, outer, inner = mixer_inputs(gathered, conv_input, outer_gate, inner_gate)
    gated_input = (inner * conv_values).reshape(seqs, -1, conv_values.shape[1])
    one_back = jnp.pad(gated_input, ((0, 0), (1, 0), (0, 0)))[:, :-1]
    two_back = jnp.pad(gated_input, ((0, 0), (2, 0), (0, 0)))[:, :-2]
    convolved = conv_taps[0] * two_back + conv_taps[1] * one_back + conv_taps[2] * gated_input
    mixed = (outer * convolved.reshape(conv_values.shape)).astype(jnp.bfloat16)
    branch = project_down(mixed, mixer_out)
    return (stream.astype(jnp.float32) + branch).astype(jnp.bfloat16)


def on_device(
    tokens,
    first_gain,
    first_gate,
    first_up,
    first_down,
    mixer_gain,
    conv_input,
    outer_gate,
    inner_gate,
    conv_taps,
    mixer_out,
    second_gain,
    second_gate,
    second_up,
    second_down,
):
    seqs, length, width = tokens.shape
    stream = tokens.reshape(seqs * length, width)
    stream = half_ffn(stream, first_gain, first_gate, first_up, first_down)
    stream = conv_mixer(
        stream, seqs, mixer_gain, conv_input, outer_gate, inner_gate, conv_taps, mixer_out
    )
    stream = half_ffn(stream, second_gain, second_gate, second_up, second_down)
    return stream.reshape(seqs, length, width)


def solution(mesh):
    in_specs = (
        P("fs", None, "tp"),
        P(),
        P("fs", "tp"),
        P("fs", "tp"),
        P("tp", "fs"),
        P(),
        P("fs", "tp"),
        P("fs", "tp"),
        P("fs", "tp"),
        P(None, "tp"),
        P("tp", "fs"),
        P(),
        P("fs", "tp"),
        P("fs", "tp"),
        P("tp", "fs"),
    )
    out_specs = P("fs", None, "tp")
    return jax.shard_map(
        on_device, mesh=mesh, in_specs=in_specs, out_specs=out_specs, check_vma=False
    )
```

profile of v0, /device:TPU:0, one launch (start us, length us, event | category | flops | bytes accessed | tf_op | source)
XLA Modules:
  0.0 947.5 jit_solution(4137865059658070734)
XLA Ops:
  6.5 0.7 all-gather.14.cloned.1.call-update
  7.3 0.0 all-gather.16.cloned.1.call-start
  7.3 0.7 all-gather.16.cloned.1.call-update
  8.0 0.0 all-gather.18.cloned.1.call-start
  8.1 0.7 all-gather.18.cloned.1.call-update
  8.7 0.0 all-gather.20.cloned.1.call-start
  8.8 0.5 all-gather.20.cloned.1.call-update
  9.3 0.0 reduce-scatter.4.cloned.1.call-start
  9.4 30.8 %all-gather.14.cloned.1.call-done = bf16[768,2048]{1,0:T(8,128)(2,1)} async-done(((bf16[768,512]{1,0:T(8,128)(2,1)}), bf16[768,2048]{1,0:T(8,128)(2,1)}) %all-gather.14.cloned.1.call-update) | async-done | bytes 3145744 | tf_op jit(solution)/shard_map/all_gather | solution.py:10
  40.2 2.6 fusion
  42.8 85.5 %all-gather.16.cloned.1.call-done = bf16[2048,1280]{1,0:T(8,128)(2,1)} async-done(((bf16[256,1280]{1,0:T(8,128)(2,1)}), bf16[2048,1280]{1,0:T(8,128)(2,1)}) %all-gather.16.cloned.1.call-update) | async-done | bytes 5242896 | tf_op jit(solution)/shard_map/all_gather | solution.py:26
  128.3 9.6 %fusion.18 = f32[768,1280]{1,0:T(8,128)} fusion(bf16[2048,1280]{1,0:T(8,128)(2,1)} %all-gather.16.cloned.1.call-done, bf16[768,2048]{1,0:T(8,128)(2,1)} %all-gather.14.cloned.1.call-done, f32[2048]{0:T(1024)S(1)} %copy-done.5, f32[768]{0:T(1024)S(1)} %add_rsqrt_fusion.2), kind=kOutput, calls=%fused_computation.29 | convolution fusion | flops 4032823296 | bytes 12332032 | tf_op jit(solution)/shard_map/dot_general | solution.py:17
  137.8 76.7 %all-gather.18.cloned.1.call-done = bf16[2048,1280]{1,0:T(8,128)(2,1)} async-done(((bf16[256,1280]{1,0:T(8,128)(2,1)}), bf16[2048,1280]{1,0:T(8,128)(2,1)}) %all-gather.18.cloned.1.call-update) | async-done | bytes 5242896 | tf_op jit(solution)/shard_map/all_gather | solution.py:27
  214.5 86.9 %all-gather.20.cloned.1.call-done = bf16[1280,2048]{1,0:T(8,128)(2,1)} async-done(((bf16[1280,256]{1,0:T(8,128)(2,1)}), bf16[1280,2048]{1,0:T(8,128)(2,1)}) %all-gather.20.cloned.1.call-update) | async-done | bytes 5242896 | tf_op jit(solution)/shard_map/all_gather | solution.py:47
  301.4 16.4 %convolution_convert_fusion.2 = bf16[768,2048]{1,0:T(8,128)(2,1)} fusion(bf16[1280,2048]{1,0:T(8,128)(2,1)} %all-gather.20.cloned.1.call-done, bf16[2048,1280]{1,0:T(8,128)(2,1)} %all-gather.18.cloned.1.call-done, f32[768,1280]{1,0:T(8,128)} %fusion.18, bf16[768,2048]{1,0:T(8,128)(2,1)S(1)} %copy-done.3, f32[2048]{0:T(1024)S(1)} %copy-done.5, ...), kind=kOutput, calls=%fused_computation.21 | convolution fusion | flops 8066826240 | bytes 20720640 | tf_op jit(solution)/shard_map/dot_general | solution.py:46
  317.8 0.0 reduce-scatter.4.cloned.1.call-update
  317.9 0.0 copy-start.6
  317.9 0.0 all-gather.22.cloned.1.call-start
  317.9 36.0 %reduce-scatter.4.cloned.1.call-done = bf16[768,512]{1,0:T(8,128)(2,1)} async-done(((bf16[768,2048]{1,0:T(8,128)(2,1)}), bf16[768,512]{1,0:T(8,128)(2,1)}) %reduce-scatter.4.cloned.1.call-update) | async-done | bytes 786448 | tf_op jit(solution)/shard_map/reduce_scatter | solution.py:49
  353.9 2.5 add_convert_fusion.2
  356.4 0.0 all-gather.22.cloned.1.call-update
  356.4 0.0 all-gather.26.cloned.1.call-start
  356.5 0.7 all-gather.26.cloned.1.call-update
  357.2 0.0 all-gather.28.cloned.1.call-start
  357.2 0.7 all-gather.28.cloned.1.call-update
  357.9 0.0 all-gather.24.cloned.1.call-start
  358.0 0.7 all-gather.24.cloned.1.call-update
  358.7 0.0 all-gather.30.cloned.1.call-start
  358.7 0.5 all-gather.30.cloned.1.call-update
  359.2 0.2 reduce-scatter.6.cloned.1.call-start
  359.5 25.6 %all-gather.22.cloned.1.call-done = bf16[768,2048]{1,0:T(8,128)(2,1)} async-done(((bf16[768,512]{1,0:T(8,128)(2,1)}), bf16[768,2048]{1,0:T(8,128)(2,1)}) %all-gather.22.cloned.1.call-update) | async-done | bytes 3145744 | tf_op jit(solution)/shard_map/all_gather | solution.py:10
  385.1 2.6 fusion.3
  387.7 0.0 copy-start.2
  387.7 39.8 %all-gather.26.cloned.1.call-done = bf16[2048,256]{1,0:T(8,128)(2,1)} async-done(((bf16[256,256]{1,0:T(8,128)(2,1)}), bf16[2048,256]{1,0:T(8,128)(2,1)}) %all-gather.26.cloned.1.call-update) | async-done | bytes 1048592 | tf_op jit(solution)/shard_map/all_gather | solution.py:41
  427.5 4.1 fusion.29
  431.6 37.0 %all-gather.28.cloned.1.call-done = bf16[2048,256]{1,0:T(8,128)(2,1)} async-done(((bf16[256,256]{1,0:T(8,128)(2,1)}), bf16[2048,256]{1,0:T(8,128)(2,1)}) %all-gather.28.cloned.1.call-update) | async-done | bytes 1048592 | tf_op jit(solution)/shard_map/all_gather | solution.py:38
  468.7 2.5 convolution_multiply_fusion.2
  471.1 0.2 fusion.24
  471.4 38.4 %all-gather.24.cloned.1.call-done = bf16[2048,256]{1,0:T(8,128)(2,1)} async-done(((bf16[256,256]{1,0:T(8,128)(2,1)}), bf16[2048,256]{1,0:T(8,128)(2,1)}) %all-gather.24.cloned.1.call-update) | async-done | bytes 1048592 | tf_op jit(solution)/shard_map/all_gather | solution.py:40
  509.8 40.0 %all-gather.30.cloned.1.call-done = bf16[256,2048]{1,0:T(8,128)(2,1)} async-done(((bf16[256,256]{1,0:T(8,128)(2,1)}), bf16[256,2048]{1,0:T(8,128)(2,1)}) %all-gather.30.cloned.1.call-update) | async-done | bytes 1048592 | tf_op jit(solution)/shard_map/all_gather | solution.py:47
  549.8 7.6 convolution_convert_fusion
  557.5 0.0 reduce-scatter.6.cloned.1.call-update
  557.5 0.0 copy-start.7
  557.5 0.0 all-gather.32.cloned.1.call-start
  557.5 36.8 %reduce-scatter.6.cloned.1.call-done = bf16[768,512]{1,0:T(8,128)(2,1)} async-done(((bf16[768,2048]{1,0:T(8,128)(2,1)}), bf16[768,512]{1,0:T(8,128)(2,1)}) %reduce-scatter.6.cloned.1.call-update) | async-done | bytes 786448 | tf_op jit(solution)/shard_map/reduce_scatter | solution.py:49
  594.4 2.2 add_convert_fusion.1
  596.6 0.0 all-gather.32.cloned.1.call-update
  596.6 0.0 all-gather.34.cloned.1.call-start
  596.7 0.7 all-gather.34.cloned.1.call-update
  597.4 0.0 all-gather.36.cloned.1.call-start
  597.4 0.5 all-gather.36.cloned.1.call-update
  598.0 0.0 all-gather.38.cloned.1.call-start
  598.0 0.5 all-gather.38.cloned.1.call-update
  598.5 0.3 reduce-scatter.8.cloned.1.call-start
  598.8 26.5 %all-gather.32.cloned.1.call-done = bf16[768,2048]{1,0:T(8,128)(2,1)} async-done(((bf16[768,512]{1,0:T(8,128)(2,1)}), bf16[768,2048]{1,0:T(8,128)(2,1)}) %all-gather.32.cloned.1.call-update) | async-done | bytes 3145744 | tf_op jit(solution)/shard_map/all_gather | solution.py:10
  625.3 2.6 fusion.6
  627.9 85.5 %all-gather.34.cloned.1.call-done = bf16[2048,1280]{1,0:T(8,128)(2,1)} async-done(((bf16[256,1280]{1,0:T(8,128)(2,1)}), bf16[2048,1280]{1,0:T(8,128)(2,1)}) %all-gather.34.cloned.1.call-update) | async-done | bytes 5242896 | tf_op jit(solution)/shard_map/all_gather | solution.py:26
  713.4 9.6 %fusion.13 = f32[768,1280]{1,0:T(8,128)} fusion(bf16[2048,1280]{1,0:T(8,128)(2,1)} %all-gather.34.cloned.1.call-done, bf16[768,2048]{1,0:T(8,128)(2,1)} %all-gather.32.cloned.1.call-done, f32[2048]{0:T(1024)S(1)} %copy-done.7, f32[768]{0:T(1024)S(1)} %add_rsqrt_fusion), kind=kOutput, calls=%fused_computation.28 | convolution fusion | flops 4032823296 | bytes 12332032 | tf_op jit(solution)/shard_map/dot_general | solution.py:17
  723.0 76.5 %all-gather.36.cloned.1.call-done = bf16[2048,1280]{1,0:T(8,128)(2,1)} async-done(((bf16[256,1280]{1,0:T(8,128)(2,1)}), bf16[2048,1280]{1,0:T(8,128)(2,1)}) %all-gather.36.cloned.1.call-update) | async-done | bytes 5242896 | tf_op jit(solution)/shard_map/all_gather | solution.py:27
  799.5 86.9 %all-gather.38.cloned.1.call-done = bf16[1280,2048]{1,0:T(8,128)(2,1)} async-done(((bf16[1280,256]{1,0:T(8,128)(2,1)}), bf16[1280,2048]{1,0:T(8,128)(2,1)}) %all-gather.38.cloned.1.call-update) | async-done | bytes 5242896 | tf_op jit(solution)/shard_map/all_gather | solution.py:47
  886.4 16.2 %convolution_convert_fusion.1 = bf16[768,2048]{1,0:T(8,128)(2,1)} fusion(bf16[1280,2048]{1,0:T(8,128)(2,1)} %all-gather.38.cloned.1.call-done, bf16[2048,1280]{1,0:T(8,128)(2,1)} %all-gather.36.cloned.1.call-done, f32[768,1280]{1,0:T(8,128)} %fusion.13, bf16[768,2048]{1,0:T(8,128)(2,1)} %all-gather.32.cloned.1.call-done, f32[2048]{0:T(1024)S(1)} %copy-done.7, ...), kind=kOutput, calls=%fused_computation.20 | convolution fusion | flops 8066826240 | bytes 20720640 | tf_op jit(solution)/shard_map/dot_general | solution.py:46
  902.6 0.0 reduce-scatter.8.cloned.1.call-update
  902.6 36.1 %reduce-scatter.8.cloned.1.call-done = bf16[768,512]{1,0:T(8,128)(2,1)} async-done(((bf16[768,2048]{1,0:T(8,128)(2,1)}), bf16[768,512]{1,0:T(8,128)(2,1)}) %reduce-scatter.8.cloned.1.call-update) | async-done | bytes 786448 | tf_op jit(solution)/shard_map/reduce_scatter | solution.py:49
  938.7 2.2 add_convert_fusion
  (18 shorter events, 0.1 us)
Async XLA Ops:
  6.5 121.7 %copy-start.5 = (f32[2048]{0:T(1024)S(1)}, f32[2048]{0:T(1024)}, u32[]{:S(2)}) copy-start(f32[2048]{0:T(1024)} %param.16) | copy-start | bytes 24580
  6.5 33.6 %all-gather.14.cloned.1.call-start = ((), (), s32[]{:S(2)}) async-start(), calls=%async_computation.3 | async-start | bytes 3932160 | tf_op jit(solution)/shard_map/all_gather | solution.py:10
  7.3 121.0 %all-gather.16.cloned.1.call-start = ((), (), s32[]{:S(2)}) async-start(), calls=%async_computation.4 | async-start | bytes 5898240 | tf_op jit(solution)/shard_map/all_gather | solution.py:26
  8.0 206.5 %all-gather.18.cloned.1.call-start = ((), (), s32[]{:S(2)}) async-start(), calls=%async_computation.5 | async-start | bytes 5898240 | tf_op jit(solution)/shard_map/all_gather | solution.py:27
  8.7 292.7 %all-gather.20.cloned.1.call-start = ((), (), s32[]{:S(2)}) async-start(), calls=%async_computation.6 | async-start | bytes 5898240 | tf_op jit(solution)/shard_map/all_gather | solution.py:47
  9.3 344.6 %reduce-scatter.4.cloned.1.call-start = ((), (), s32[]{:S(2)}) async-start(), calls=%async_computation.7 | async-start | bytes 3932160 | tf_op jit(solution)/shard_map/reduce_scatter | solution.py:49
  42.7 258.7 %copy-start.3 = (bf16[768,2048]{1,0:T(8,128)(2,1)S(1)}, bf16[768,2048]{1,0:T(8,128)(2,1)}, u32[]{:S(2)}) copy-start(bf16[768,2048]{1,0:T(8,128)(2,1)} %all-gather.14.cloned.1.call-done) | copy-start | bytes 9437188
  317.8 41.6 %copy-start.4 = (f32[3,256]{1,0:T(4,128)S(1)}, f32[3,256]{1,0:T(4,128)}, u32[]{:S(2)}) copy-start(f32[3,256]{1,0:T(4,128)} %param.24) | copy-start | bytes 9220
  317.9 109.6 %copy-start.6 = (f32[2048]{0:T(1024)S(1)}, f32[2048]{0:T(1024)}, u32[]{:S(2)}) copy-start(f32[2048]{0:T(1024)} %param.20) | copy-start | bytes 24580
  317.9 67.2 %all-gather.22.cloned.1.call-start = ((), (), s32[]{:S(2)}) async-start(), calls=%async_computation.8 | async-start | bytes 3932160 | tf_op jit(solution)/shard_map/all_gather | solution.py:10
  356.4 71.1 %all-gather.26.cloned.1.call-start = ((), (), s32[]{:S(2)}) async-start(), calls=%async_computation.10 | async-start | bytes 1179648 | tf_op jit(solution)/shard_map/all_gather | solution.py:41
  357.2 111.5 %all-gather.28.cloned.1.call-start = ((), (), s32[]{:S(2)}) async-start(), calls=%async_computation.11 | async-start | bytes 1179648 | tf_op jit(solution)/shard_map/all_gather | solution.py:38
  357.9 151.9 %all-gather.24.cloned.1.call-start = ((), (), s32[]{:S(2)}) async-start(), calls=%async_computation.9 | async-start | bytes 1179648 | tf_op jit(solution)/shard_map/all_gather | solution.py:40
  358.7 191.2 %all-gather.30.cloned.1.call-start = ((), (), s32[]{:S(2)}) async-start(), calls=%async_computation.12 | async-start | bytes 1179648 | tf_op jit(solution)/shard_map/all_gather | solution.py:47
  359.2 235.1 %reduce-scatter.6.cloned.1.call-start = ((), (), s32[]{:S(2)}) async-start(), calls=%async_computation.13 | async-start | bytes 3932160 | tf_op jit(solution)/shard_map/reduce_scatter | solution.py:49
  387.7 81.0 %copy-start.2 = (bf16[768,2048]{1,0:T(8,128)(2,1)S(1)}, bf16[768,2048]{1,0:T(8,128)(2,1)}, u32[]{:S(2)}) copy-start(bf16[768,2048]{1,0:T(8,128)(2,1)} %all-gather.22.cloned.1.call-done) | copy-start | bytes 9437188
  549.8 44.5 %copy-start = (bf16[768,512]{1,0:T(8,128)(2,1)S(1)}, bf16[768,512]{1,0:T(8,128)(2,1)}, u32[]{:S(2)}) copy-start(bf16[768,512]{1,0:T(8,128)(2,1)} %add_convert_fusion.2) | copy-start | bytes 2359300
  557.5 155.9 %copy-start.7 = (f32[2048]{0:T(1024)S(1)}, f32[2048]{0:T(1024)}, u32[]{:S(2)}) copy-start(f32[2048]{0:T(1024)} %param.26) | copy-start | bytes 24580
  557.5 67.8 %all-gather.32.cloned.1.call-start = ((), (), s32[]{:S(2)}) async-start(), calls=%async_computation.14 | async-start | bytes 3932160 | tf_op jit(solution)/shard_map/all_gather | solution.py:10
  596.6 116.8 %all-gather.34.cloned.1.call-start = ((), (), s32[]{:S(2)}) async-start(), calls=%async_computation.15 | async-start | bytes 5898240 | tf_op jit(solution)/shard_map/all_gather | solution.py:26
  597.4 202.1 %all-gather.36.cloned.1.call-start = ((), (), s32[]{:S(2)}) async-start(), calls=%async_computation.16 | async-start | bytes 5898240 | tf_op jit(solution)/shard_map/all_gather | solution.py:27
  598.0 288.4 %all-gather.38.cloned.1.call-start = ((), (), s32[]{:S(2)}) async-start(), calls=%async_computation.17 | async-start | bytes 5898240 | tf_op jit(solution)/shard_map/all_gather | solution.py:47
  598.5 340.2 %reduce-scatter.8.cloned.1.call-start = ((), (), s32[]{:S(2)}) async-start(), calls=%async_computation.18 | async-start | bytes 3932160 | tf_op jit(solution)/shard_map/reduce_scatter | solution.py:49
  723.0 215.7 %copy-start.1 = (bf16[768,512]{1,0:T(8,128)(2,1)S(1)}, bf16[768,512]{1,0:T(8,128)(2,1)}, u32[]{:S(2)}) copy-start(bf16[768,512]{1,0:T(8,128)(2,1)} %add_convert_fusion.1) | copy-start | bytes 2359300
Sparse Core Ops, SparseCore 0:
  8.9 31.2 all-gather.13
  42.3 85.8 all-gather.15
  130.4 84.0 all-gather.17
  216.4 84.9 all-gather.19
  318.0 35.8 reduce-scatter.3
  356.5 28.4 all-gather.21
  387.2 40.2 all-gather.25
  429.6 38.9 all-gather.27
  470.8 38.9 all-gather.23
  511.7 38.0 all-gather.29
  557.6 36.7 reduce-scatter.5
  596.7 28.5 all-gather.31
  627.5 85.8 all-gather.33
  715.4 84.0 all-gather.35
  801.4 84.9 all-gather.37
  902.8 35.8 reduce-scatter.7
where the time goes:
time: 948 us; the launch traced here: 947 us
  waiting for transfers between devices  852 us (90%)
  matrix products  66 us (7%)
  other arithmetic  14.9 us (2%)
  between operations  13.4 us (1%)
    all_gather x3, waiting for transfers between devices, project_down(): lax.all_gather(weight, 'fs', axis=1, tiled=True)  214 us
    all_gather x2, waiting for transfers between devices, ffn_inputs(): lax.all_gather(gate_weight, 'fs', axis=0, tiled=True)  171 us
    all_gather x2, waiting for transfers between devices, ffn_inputs(): lax.all_gather(up_weight, 'fs', axis=0, tiled=True)  153 us
    reduce_scatter x3, waiting for transfers between devices, project_down(): lax.psum_scatter(partial_sum.astype(jnp.bfloat16), 'tp', scatter_dimensio...  109 us
    all_gather x3, waiting for transfers between devices, norm_rows(): whole = lax.all_gather(stream, 'tp', axis=1, tiled=True)  82.9 us
    dot_general x3, matrix products, project_down(): jnp.dot(hidden, lax.all_gather(weight, 'fs', axis=1, tiled=True), preferr...  40.2 us
    all_gather x1, waiting for transfers between devices, mixer_inputs(): lax.all_gather(inner_gate, 'fs', axis=0, tiled=True)  39.8 us
    all_gather x1, waiting for transfers between devices, mixer_inputs(): lax.all_gather(outer_gate, 'fs', axis=0, tiled=True)  38.4 us
  transfers between devices with their start and end apart: 16, of which 16 were waited for; matrix products, arithmetic and copies ran while one was open for 4% of the time, Pallas kernels for 0%

commit v1 on v0

v1 whole, which is shorter than its diff:
```python
import functools

import jax
import jax.numpy as jnp
from jax import lax
from jax.experimental import pallas as pl
from jax.experimental.pallas import tpu as pltpu
from jax.sharding import PartitionSpec as P

epsilon = 1e-05
MESH = pl.DeviceIdType.MESH
UP, DOWN, ACROSS = 0, 1, 2


def tile_of(columns):
    return 256 if columns % 256 == 0 else 128


def when(condition):
    return pl.when(condition)


def layer_kernel(n_fs, n_tp, seqs, length, n_late, *refs):
    tokens, first_gain, mixer_gain, second_gain, conv_taps = refs[:5]
    shards = refs[5:14]
    late_shard = refs[14]
    out_ref = refs[15]
    wholes = refs[16:25]
    late_whole, blocks, normed, hidden, partial, arrived = refs[25:31]
    (
        load_sem, send_sem, recv_sem, late_send, late_recv,
        gather_send, gather_recv, scatter_send, scatter_recv, token_sem,
    ) = refs[31:]
    n_early = len(shards)
    rows = seqs * length
    line = n_fs // 2

    me = lax.axis_index("fs")
    z, x = me // 2, lax.rem(me, 2)
    above, below, beside = me + 2, me - 2, me + 1 - 2 * x
    has_above, has_below = z + 1 < line, z >= 1
    t = lax.axis_index("tp")
    pair = t + 1 - 2 * lax.rem(t, 2)
    chips = n_tp // 2
    facing = [lax.rem(t + 2 * d, n_tp) for d in range(chips)]
    diagonal = [lax.rem(pair + 2 * d, n_tp) for d in range(chips)]
    others = range(1, chips)

    token_copy = pltpu.make_async_copy(tokens, blocks.at[0, t], token_sem)
    token_copy.start()
    loads = [
        pltpu.make_async_copy(shards[m], wholes[m].at[me], load_sem.at[m]) for m in range(n_early)
    ]
    depth = late_shard.shape[0] // n_late
    late_load = pltpu.make_async_copy(late_shard, late_whole.at[me], load_sem.at[n_early])
    for load in loads:
        load.start()
    late_load.start()

    barrier = pltpu.get_barrier_semaphore()

    def greet(axis, device):
        pl.semaphore_signal(barrier, inc=1, device_id={axis: device}, device_id_type=MESH)

    greet("tp", pair)
    for d in others:
        greet("tp", facing[d])
    greet("fs", beside)
    when(has_above)(lambda: greet("fs", above))
    when(has_below)(lambda: greet("fs", below))
    pl.semaphore_wait(
        barrier, chips + 1 + has_above.astype(jnp.int32) + has_below.astype(jnp.int32)
    )

    def early_copy(m, origin, way):
        return pltpu.make_async_remote_copy(
            src_ref=wholes[m].at[origin],
            dst_ref=wholes[m].at[origin],
            send_sem=send_sem.at[m, origin, way],
            recv_sem=recv_sem.at[m, origin],
            device_id={"fs": (above, below, beside)[way]},
            device_id_type=MESH,
        )

    def late_copy(k, origin, way):
        part = pl.ds(k * depth, depth)
        return pltpu.make_async_remote_copy(
            src_ref=late_whole.at[origin, part],
            dst_ref=late_whole.at[origin, part],
            send_sem=late_send.at[k, origin, way],
            recv_sem=late_recv.at[k, origin],
            device_id={"fs": (above, below, beside)[way]},
            device_id_type=MESH,
        )

    def early_own(m):
        loads[m].wait()
        early_copy(m, me, ACROSS).start()
        when(has_above)(lambda: early_copy(m, me, UP).start())
        when(has_below)(lambda: early_copy(m, me, DOWN).start())

    def early_step(m, step):
        @when(z >= step)
        def _():
            origin = me - 2 * step
            early_copy(m, origin, ACROSS).wait_recv()
            when(has_above)(lambda: early_copy(m, origin, UP).start())
            early_copy(m, origin, ACROSS).start()

        @when(z + step < line)
        def _():
            origin = me + 2 * step
            early_copy(m, origin, ACROSS).wait_recv()
            when(has_below)(lambda: early_copy(m, origin, DOWN).start())
            early_copy(m, origin, ACROSS).start()

    def early_across(m):
        for at in range(line):
            early_copy(m, 2 * at + 1 - x, ACROSS).wait_recv()

    def late_own(k):
        if k == 0:
            late_load.wait()
        late_copy(k, me, ACROSS).start()
        when(has_above)(lambda: late_copy(k, me, UP).start())
        when(has_below)(lambda: late_copy(k, me, DOWN).start())

    def late_across(k):
        late_copy(k, beside, ACROSS).wait_recv()
        when(has_above)(lambda: late_copy(k, beside, UP).start())
        when(has_below)(lambda: late_copy(k, beside, DOWN).start())

    def late_step(k, step):
        @when(z >= step)
        def _():
            for column in (me, beside):
                origin = column - 2 * step
                late_copy(k, origin, ACROSS).wait_recv()
                when(has_above)(functools.partial(lambda o: late_copy(k, o, UP).start(), origin))

        @when(z + step < line)
        def _():
            for column in (me, beside):
                origin = column + 2 * step
                late_copy(k, origin, ACROSS).wait_recv()
                when(has_below)(functools.partial(lambda o: late_copy(k, o, DOWN).start(), origin))

    def drain():
        for at in range(line):
            own_column = 2 * at + x
            for m in range(n_early):
                early_copy(m, own_column, ACROSS).wait_send()

            @when(jnp.logical_and(at <= z, has_above))
            def _():
                for m in range(n_early):
                    early_copy(m, own_column, UP).wait_send()
                for k in range(n_late):
                    for column in range(2):
                        late_copy(k, 2 * at + column, UP).wait_send()

            @when(jnp.logical_and(at >= z, has_below))
            def _():
                for m in range(n_early):
                    early_copy(m, own_column, DOWN).wait_send()
                for k in range(n_late):
                    for column in range(2):
                        late_copy(k, 2 * at + column, DOWN).wait_send()

        for k in range(n_late):
            late_copy(k, me, ACROSS).wait_send()

    def gather_copy(phase, block, way):
        target = pair if way == 0 or way >= chips else facing[way]
        return pltpu.make_async_remote_copy(
            src_ref=blocks.at[phase, block],
            dst_ref=blocks.at[phase, block],
            send_sem=gather_send.at[phase, way],
            recv_sem=gather_recv.at[phase, block],
            device_id={"tp": target},
            device_id_type=MESH,
        )

    def gather_start(phase):
        for d in others:
            gather_copy(phase, t, d).start()
        gather_copy(phase, t, 0).start()

    def gather_forward(phase):
        for d in others:
            gather_copy(phase, facing[d], d).wait_recv()
            gather_copy(phase, facing[d], chips + d - 1).start()

    def gather_finish(phase):
        gather_copy(phase, pair, 0).wait_recv()
        gather_copy(phase, t, 0).wait_send()
        for d in others:
            gather_copy(phase, diagonal[d], 0).wait_recv()
            gather_copy(phase, t, d).wait_send()
            gather_copy(phase, facing[d], chips + d - 1).wait_send()

    def scatter_copy(phase, way):
        block = diagonal[way] if way < chips else facing[way - chips + 1]
        target = pair if way < chips else facing[way - chips + 1]
        return pltpu.make_async_remote_copy(
            src_ref=partial.at[block],
            dst_ref=arrived.at[phase, way],
            send_sem=scatter_send.at[phase, way],
            recv_sem=scatter_recv.at[phase, way],
            device_id={"tp": target},
            device_id_type=MESH,
        )

    chunk = length // 3

    def row_loop(body):
        @pl.loop(0, rows // chunk)
        def _(i):
            body(pl.ds(pl.multiple_of(i * chunk, chunk), chunk))

    def scatter_start(phase):
        for d in others:
            scatter_copy(phase, d).start()
        scatter_copy(phase, 0).start()

    def scatter_middle(phase):
        for d in others:
            scatter_copy(phase, d).wait_recv()
            block = facing[d]

            def body(at):
                total = partial[block, at, :].astype(jnp.float32) + arrived[
                    phase, d, at, :
                ].astype(jnp.float32)
                partial[block, at, :] = total.astype(jnp.bfloat16)

            row_loop(body)
            scatter_copy(phase, chips + d - 1).start()

    def scatter_finish(phase, scale):
        scatter_copy(phase, 0).wait_recv()
        for d in others:
            scatter_copy(phase, chips + d - 1).wait_recv()

        def body(at):
            branch = partial[t, at, :].astype(jnp.float32)
            for way in [0] + [chips + d - 1 for d in others]:
                branch = branch + arrived[phase, way, at, :].astype(jnp.float32)
            value = (blocks[phase, t, at, :].astype(jnp.float32) + scale * branch).astype(
                jnp.bfloat16
            )
            if phase == 2:
                out_ref[at, :] = value
            else:
                blocks[phase + 1, t, at, :] = value

        row_loop(body)
        for way in range(2 * chips - 1):
            scatter_copy(phase, way).wait_send()

    width = tokens.shape[1]

    def norm(phase, gain):
        def body(at):
            values = [blocks[phase, b, at, :].astype(jnp.float32) for b in range(n_tp)]
            squares = sum(jnp.sum(v * v, axis=1, keepdims=True) for v in values)
            scale = lax.rsqrt(squares / (width * n_tp) + epsilon)
            for b, v in enumerate(values):
                cols = pl.ds(b * width, width)
                normed[at, cols] = (v * scale * gain[:, cols]).astype(jnp.bfloat16)

        row_loop(body)

    def times(at, m, cols):
        weight = wholes[m][:, :, cols]
        weight = weight.reshape(weight.shape[0] * weight.shape[1], weight.shape[2])
        return jnp.dot(normed[at, :], weight, preferred_element_type=jnp.float32)

    def ffn_inputs(gate, upward):
        tile = tile_of(wholes[gate].shape[2])

        @pl.loop(0, wholes[gate].shape[2] // tile)
        def _(n):
            cols = pl.ds(pl.multiple_of(n * tile, tile), tile)

            @pl.loop(0, seqs)
            def _(s):
                at = pl.ds(pl.multiple_of(s * length, length), length)
                g = times(at, gate, cols)
                g = g / (1.0 + jnp.exp(-g))
                hidden[at, cols] = (g * times(at, upward, cols)).astype(jnp.bfloat16)

    def project_down(whole):
        inner, piece = whole.shape[1:]
        per_block = width // piece

        @pl.loop(0, n_fs)
        def _(j):
            block = j // per_block
            cols = pl.ds(pl.multiple_of(lax.rem(j, per_block) * piece, piece), piece)

            @pl.loop(0, seqs)
            def _(s):
                at = pl.ds(pl.multiple_of(s * length, length), length)
                product = jnp.dot(
                    hidden[at, :inner], whole[j], preferred_element_type=jnp.float32
                )
                partial[block, at, cols] = product.astype(jnp.bfloat16)

    def mixer_inputs(conv_input, outer_gate, inner_gate):
        tile = tile_of(wholes[conv_input].shape[2])

        @pl.loop(0, wholes[conv_input].shape[2] // tile)
        def _(n):
            cols = pl.ds(pl.multiple_of(n * tile, tile), tile)
            taps = conv_taps[:, cols]
            position = lax.broadcasted_iota(jnp.int32, (length, tile), 0)

            @pl.loop(0, seqs)
            def _(s):
                at = pl.ds(pl.multiple_of(s * length, length), length)
                gated = times(at, inner_gate, cols) * times(at, conv_input, cols)
                one_back = jnp.where(position >= 1, pltpu.roll(gated, 1, 0), 0.0)
                two_back = jnp.where(position >= 2, pltpu.roll(gated, 2, 0), 0.0)
                convolved = taps[0:1] * two_back + taps[1:2] * one_back + taps[2:3] * gated
                hidden[at, cols] = (times(at, outer_gate, cols) * convolved).astype(jnp.bfloat16)

    units = [("e", 0), ("l", 0), ("e", 1), ("l", 1), ("e", 2), ("l", 2), ("e", 3), ("e", 4)]
    units += [("e", 5), ("e", 6), ("l", 3), ("e", 7), ("l", 4), ("e", 8)]
    ahead = 4

    def own(index):
        if index < len(units):
            kind, which = units[index]
            (early_own if kind == "e" else late_own)(which)

    def after_step(m, step):
        if m == 0 and step == 1:
            gather_forward(0)
        if m == 7:
            if step == 1:
                scatter_middle(1)
            if step == 2:
                scatter_finish(1, 1.0)
                gather_start(2)
            if step == 3:
                gather_forward(2)
        if m == 8 and step == 1:
            gather_finish(2)
            norm(2, second_gain)

    def after_unit(m):
        if m == 0:
            gather_finish(0)
            norm(0, first_gain)
        if m == 1:
            ffn_inputs(0, 1)
        if m == 2:
            project_down(wholes[2])
            scatter_start(0)
        if m == 3:
            scatter_middle(0)
        if m == 4:
            scatter_finish(0, 0.5)
            gather_start(1)
        if m == 5:
            gather_forward(1)
        if m == 6:
            gather_finish(1)
            norm(1, mixer_gain)
            mixer_inputs(3, 4, 5)
            project_down(wholes[6])
            scatter_start(1)
        if m == 8:
            ffn_inputs(7, 8)
            project_down(late_whole)
            scatter_start(2)
            scatter_middle(2)
            scatter_finish(2, 0.5)

    token_copy.wait()
    for index in range(ahead):
        own(index)
        if index == 0:
            gather_start(0)
    for index, (kind, which) in enumerate(units):
        if kind == "l":
            late_across(which)
        for step in range(1, line):
            if kind == "e":
                early_step(which, step)
                if step <= 3:
                    after_step(which, step)
            else:
                late_step(which, step)
        own(index + ahead)
        if kind == "e":
            early_across(which)
            after_unit(which)
    drain()


def on_device(n_fs, n_tp, *args):
    (
        tokens, first_gain, first_gate, first_up, first_down, mixer_gain, conv_input, outer_gate,
        inner_gate, conv_taps, mixer_out, second_gain, second_gate, second_up, second_down,
    ) = args
    seqs, length, width = tokens.shape
    rows, model = seqs * length, width * n_tp
    shards = (
        first_gate, first_up, first_down, conv_input, outer_gate, inner_gate, mixer_out,
        second_gate, second_up,
    )
    n_late = 5 if second_down.shape[0] % 80 == 0 else 1
    in_hbm = pl.BlockSpec(memory_space=pl.ANY)
    in_vmem = pl.BlockSpec(memory_space=pltpu.VMEM)
    half = jnp.bfloat16
    dma = pltpu.SemaphoreType.DMA
    scratch = [pltpu.VMEM((n_fs,) + shard.shape, half) for shard in shards]
    scratch += [
        pltpu.VMEM((n_fs,) + second_down.shape, half),
        pltpu.VMEM((3, n_tp, rows, width), half),
        pltpu.VMEM((rows, model), half),
        pltpu.VMEM((rows, first_gate.shape[1]), half),
        pltpu.VMEM((n_tp, rows, width), half),
        pltpu.VMEM((3, n_tp - 1, rows, width), half),
        dma((len(shards) + 1,)),
        dma((len(shards), n_fs, 3)),
        dma((len(shards), n_fs)),
        dma((n_late, n_fs, 3)),
        dma((n_late, n_fs)),
        dma((3, n_tp - 1)),
        dma((3, n_tp)),
        dma((3, n_tp - 1)),
        dma((3, n_tp - 1)),
        dma,
    ]
    flops = 2 * rows * model * (6 * first_gate.shape[1] + 4 * conv_input.shape[1])
    out = pl.pallas_call(
        functools.partial(layer_kernel, n_fs, n_tp, seqs, length, n_late),
        out_shape=jax.ShapeDtypeStruct((rows, width), half),
        in_specs=[in_hbm] + [in_vmem] * 4 + [in_hbm] * 10,
        out_specs=in_vmem,
        scratch_shapes=scratch,
        compiler_params=pltpu.CompilerParams(
            collective_id=0, has_side_effects=True, vmem_limit_bytes=67043328
        ),
        cost_estimate=pl.CostEstimate(flops=flops, bytes_accessed=0, transcendentals=0),
        name="whole_layer",
    )(
        tokens.reshape(rows, width),
        first_gain.reshape(1, model),
        mixer_gain.reshape(1, model),
        second_gain.reshape(1, model),
        conv_taps,
        *shards,
        second_down,
    )
    return out.reshape(seqs, length, width)


def solution(mesh):
    in_specs = (
        P("fs", None, "tp"),
        P(),
        P("fs", "tp"),
        P("fs", "tp"),
        P("tp", "fs"),
        P(),
        P("fs", "tp"),
        P("fs", "tp"),
        P("fs", "tp"),
        P(None, "tp"),
        P("tp", "fs"),
        P(),
        P("fs", "tp"),
        P("fs", "tp"),
        P("tp", "fs"),
    )
    body = functools.partial(on_device, mesh.shape["fs"], mesh.shape["tp"])
    return jax.shard_map(
        body, mesh=mesh, in_specs=in_specs, out_specs=P("fs", None, "tp"), check_vma=False
    )
```

time: 948 us -> 456 us (0.48)
  waiting for transfers between devices: 852 us -> 0 us
  Pallas kernels: 0 us -> 453 us
  matrix products: 66 us -> 0 us
  other arithmetic: 14.9 us -> 0 us
  between operations: 13.4 us -> 0.01 us
    all_gather x13 -> x0, waiting for transfers between devices: 736 us -> none  [the longest x3 214 us: project_down(): lax.all_gather(weight, 'fs', axis=1, tiled=True)]
    pallas_call x0 -> x1, Pallas kernels: none -> 453 us  [on_device(): pl.pallas_call(functools.partial(layer_kernel, n_fs, n_tp, seqs, length,...]
    reduce_scatter x3 -> x0, waiting for transfers between devices: 109 us -> none  [project_down(): lax.psum_scatter(partial_sum.astype(jnp.bfloat16), 'tp', scatter_dimensio...]
    dot_general x7 -> x0, matrix products: 66 us -> none  [the longest x3 40.2 us: project_down(): jnp.dot(hidden, lax.all_gather(weight, 'fs', axis=1, tiled=True), preferr...]
  transfers between devices with their start and end apart: 16 -> 0, of which waited for: 16 -> 0; matrix products, arithmetic and copies ran while one was open for 4% -> 0% of each run, Pallas kernels for 0% -> 0%
where the time goes in v1:
time: 456 us; the launch traced here: 455 us
  Pallas kernels  453 us (99%)
    pallas_call x1, Pallas kernels, on_device(): pl.pallas_call(functools.partial(layer_kernel, n_fs, n_tp, seqs, length,...  453 us

profile of v1, /device:TPU:0, one launch (start us, length us, event | category | flops | bytes accessed | tf_op | source)
XLA Modules:
  0.0 455.2 jit_solution(2662544206489906979)
XLA Ops:
  0.0 453.1 %whole_layer.1 = bf16[768,512]{1,0:T(8,128)(2,1)} custom-call(bf16[768,512]{1,0:T(8,128)(2,1)} %bitcast.6, f32[1,2048]{1,0:T(1,128)} %bitcast.7, f32[1,2048]{1,0:T(1,128)} %bitcast.8, f32[1,2048]{1,0:T(1,128)} %bitcast.9, f32[3,256]{1,0:T(4,128)} %refs_4_.1, bf16[256,1280]{1,0:T(8,128)(2,1)} %refs_5_.1, bf16[256,1280]{1,0:T(8,128)(2,1)} %refs_6_.1, ...), custom_call_target="tpu_custom_call" | custom-call | flops 27380416512 | tf_op jit(solution)/shard_map/whole_layer/pallas_call | solution.py:439
  453.1 2.1 copy.17
